TPU v7x, 32 devices: a whole 2x2x4 slice. The times are simulated.
32 devices in a mesh: ep: 16 (over z, y, x), tp: 2 (over core).
Axes of the slice: x: 2, y: 2, z: 4, core: 2. Of those that a mesh axis runs over, the one named last changes fastest.
Arguments:
- tokens: bfloat16 [512, 4096], P('ep', 'tp')
- norm_gain: float32 [4096], P('tp'), may hold values from 0.1 to 1.9
- routes: int32 [512, 8], P('ep'), may hold values from 0 to 15, all different within a row; in each aligned block of 32 rows (0 to 31, 32 to 63, ...) at most 24 rows name the same one
- route_weights: float32 [512, 8], P('ep'), may hold values from 0.1 to 1
- gate_proj: bfloat16 [16, 4096, 1024], P('ep', 'tp'), may hold values from -0.09375 to 0.09375
- up_proj: bfloat16 [16, 4096, 1024], P('ep', 'tp'), may hold values from -0.09375 to 0.09375
- down_proj: bfloat16 [16, 1024, 4096], P('ep', None, 'tp')
- shared_gate: bfloat16 [4096, 1024], P('tp'), may hold values from -0.09375 to 0.09375
- shared_up: bfloat16 [4096, 1024], P('tp'), may hold values from -0.09375 to 0.09375
- shared_down: bfloat16 [1024, 4096], P(None, 'tp')
- out_gain: float32 [4096], P('tp'), may hold values from 0.1 to 1.9
Outputs:
- mixed_out: bfloat16 [512, 4096], P('ep', 'tp')
Inputs may be any that keep to these rules, and one draw needn't show every extreme that they name: `routes`: among the 32 rows of one device no expert is named more than 24 times, and in every draw some expert is named exactly 24 times by the rows of some device.
All inputs are finite; a program needn't handle non-finite values.
Results may differ from a plain program's by a relative error of at most 0.028.
Values may be sent and summed in bfloat16 or wider, within the bound.
A program may use at most 64 MiB of HBM per device.

v0:
```python
import jax
import jax.numpy as jnp
from jax import lax
from jax.sharding import PartitionSpec as P

D = 4096


def per_device(
    tokens,
    norm_gain,
    routes,
    route_weights,
    gate_proj,
    up_proj,
    down_proj,
    shared_gate,
    shared_up,
    shared_down,
    out_gain,
):
    tokens_f = tokens.astype(jnp.float32)
    squares = lax.psum(jnp.sum(tokens_f * tokens_f, axis=1), "tp")
    normed = (tokens_f * lax.rsqrt(squares / D + 1e-06)[:, None] * norm_gain[None, :]).astype(
        jnp.bfloat16
    )
    tok_rows, picks = routes.shape
    feat_local = tokens.shape[1]
    sources = lax.axis_size("ep")
    exp_local = gate_proj.shape[0]
    experts_all = sources * exp_local
    capacity = min(
        tok_rows, max(2, (3 * tok_rows * picks + 2 * experts_all - 1) // (2 * experts_all))
    )
    chosen = routes.reshape(-1)
    assigned = chosen.shape[0]
    earlier = jnp.arange(assigned)[None, :] < jnp.arange(assigned)[:, None]
    matches = (chosen[:, None] == chosen[None, :]) & earlier
    slot_rank = jnp.sum(matches.astype(jnp.int32), axis=1)
    slot_index = chosen * capacity + slot_rank
    source_rows = jnp.repeat(normed, picks, axis=0)
    outgoing = (
        jnp.zeros((experts_all * capacity, feat_local), jnp.bfloat16)
        .at[slot_index]
        .set(source_rows)
    )
    outgoing = outgoing.reshape(sources, exp_local, capacity, feat_local)
    arrived = lax.all_to_all(outgoing, "ep", split_axis=0, concat_axis=0, tiled=True)
    gate_part = jnp.einsum("sjcd,jdf->sjcf", arrived, gate_proj, preferred_element_type=jnp.float32)
    up_part = jnp.einsum("sjcd,jdf->sjcf", arrived, up_proj, preferred_element_type=jnp.float32)
    shared_gate_part = jnp.dot(normed, shared_gate, preferred_element_type=jnp.float32).reshape(
        1, 1, tok_rows, -1
    )
    shared_up_part = jnp.dot(normed, shared_up, preferred_element_type=jnp.float32).reshape(
        1, 1, tok_rows, -1
    )
    gate_pre, up_pre, shared_gate_pre, shared_up_pre = (
        lax.psum_scatter(
            gate_part.astype(jnp.bfloat16), "tp", scatter_dimension=3, tiled=True
        ).astype(jnp.float32),
        lax.psum_scatter(
            up_part.astype(jnp.bfloat16), "tp", scatter_dimension=3, tiled=True
        ).astype(jnp.float32),
        lax.psum_scatter(
            shared_gate_part.astype(jnp.bfloat16), "tp", scatter_dimension=3, tiled=True
        ).astype(jnp.float32),
        lax.psum_scatter(
            shared_up_part.astype(jnp.bfloat16), "tp", scatter_dimension=3, tiled=True
        ).astype(jnp.float32),
    )
    hidden_piece = (jax.nn.silu(gate_pre) * up_pre).astype(jnp.bfloat16)
    shared_piece = (jax.nn.silu(shared_gate_pre) * shared_up_pre).astype(jnp.bfloat16)
    hidden, shared_hidden = (
        lax.all_gather(hidden_piece, "tp", axis=3, tiled=True),
        lax.all_gather(shared_piece, "tp", axis=3, tiled=True),
    )
    expert_rows = jnp.einsum(
        "sjcf,jfd->sjcd", hidden, down_proj, preferred_element_type=jnp.float32
    ).astype(jnp.bfloat16)
    returned = lax.all_to_all(expert_rows, "ep", split_axis=0, concat_axis=0, tiled=True)
    returned = returned.reshape(experts_all * capacity, feat_local)
    gathered = returned[slot_index].astype(jnp.float32).reshape(tok_rows, picks, feat_local)
    routed = jnp.sum(gathered * route_weights[:, :, None], axis=1)
    shared_part = jnp.dot(
        shared_hidden.reshape(tok_rows, -1), shared_down, preferred_element_type=jnp.float32
    )
    mixed = shared_part + routed
    final_squares = lax.psum(jnp.sum(mixed * mixed, axis=1), "tp")
    return (mixed * lax.rsqrt(final_squares / D + 1e-06)[:, None] * out_gain[None, :]).astype(
        jnp.bfloat16
    )


def solution(mesh):
    return jax.shard_map(
        per_device,
        mesh=mesh,
        in_specs=(
            P("ep", "tp"),
            P("tp"),
            P("ep", None),
            P("ep", None),
            P("ep", "tp", None),
            P("ep", "tp", None),
            P("ep", None, "tp"),
            P("tp", None),
            P("tp", None),
            P(None, "tp"),
            P("tp"),
        ),
        out_specs=P("ep", "tp"),
        check_vma=False,
    )
```

profile of v0, /device:TPU:13, one launch (start us, length us, event | category | flops | bytes accessed | tf_op | source)
XLA Modules:
  0.0 152.1 jit_solution(2235207952409114290)
XLA Ops:
  8.0 1.0 fusion.47
  9.0 2.8 %psum.14 = f32[32]{0:T(128)S(1)} all-reduce(f32[32]{0:T(128)S(1)} %fusion.47), channel_id=1, replica_groups=mesh['ep'=16,'tp'=2] {'tp'}, use_global_device_ids=true, to_apply=%region_1.0 | all-reduce | flops 32 | bytes 256 | tf_op jit(solution)/shard_map/psum | solution.py:23
  12.3 1.0 fusion.49
  13.3 2.6 %scatter_custom_fusion = bf16[384,2048]{1,0:T(8,128)(2,1)S(1)} fusion(s32[256]{0:T(256)S(1)} %bitcast.87, bf16[]{:T(256)} %constant.6.clone.1, bf16[32,2048]{1,0:T(8,128)(2,1)S(1)} %fusion.49), kind=kCustom, calls=%fused_computation.23 | custom fusion | bytes 1703938 | tf_op jit(solution)/shard_map/scatter | solution.py:45
  15.9 42.3 %all_to_all.10 = bf16[16,1,24,2048]{3,2,1,0:T(8,128)(2,1)S(1)} all-to-all(bf16[16,1,24,2048]{3,2,1,0:T(8,128)(2,1)S(1)} %bitcast.86), channel_id=1, replica_groups=mesh['ep'=16,'tp'=2] {'ep'}, dimensions={0} | all-to-all | bytes 3145728 | tf_op jit(solution)/shard_map/all_to_all | solution.py:48
  58.3 4.9 %fusion.30 = bf16[16,1,24,1024]{3,2,0,1:T(8,128)(2,1)} fusion(bf16[1,2048,1024]{2,1,0:T(8,128)(2,1)} %param.15, bf16[16,1,24,2048]{3,2,1,0:T(8,128)(2,1)S(1)} %all_to_all.10), kind=kOutput, calls=%fused_computation.18 | convolution fusion | flops 1611005952 | bytes 6553600 | tf_op jit(solution)/shard_map/sjcd,jdf->sjcf/dot_general | solution.py:49
  63.2 4.9 %fusion.25 = bf16[16,1,24,1024]{3,2,0,1:T(8,128)(2,1)} fusion(bf16[1,2048,1024]{2,1,0:T(8,128)(2,1)} %param.16, bf16[16,1,24,2048]{3,2,1,0:T(8,128)(2,1)S(1)} %all_to_all.10), kind=kOutput, calls=%fused_computation.17 | convolution fusion | flops 1611005952 | bytes 6553600 | tf_op jit(solution)/shard_map/sjcd,jdf->sjcf/dot_general | solution.py:50
  68.1 4.2 %reduce-scatter.9.cloned.1.call-done = bf16[16,1,24,512]{3,2,0,1:T(8,128)(2,1)} async-done(((bf16[16,1,24,1024]{3,2,0,1:T(8,128)(2,1)}), bf16[16,1,24,512]{3,2,0,1:T(8,128)(2,1)}) %reduce-scatter.9.cloned.1.call-update) | async-done | bytes 393232 | tf_op jit(solution)/shard_map/reduce_scatter | solution.py:58
  72.3 11.6 %reduce-scatter.11.cloned.1.call-done = bf16[16,1,24,512]{3,2,0,1:T(8,128)(2,1)} async-done(((bf16[16,1,24,1024]{3,2,0,1:T(8,128)(2,1)}), bf16[16,1,24,512]{3,2,0,1:T(8,128)(2,1)}) %reduce-scatter.11.cloned.1.call-update) | async-done | bytes 393232 | tf_op jit(solution)/shard_map/reduce_scatter | solution.py:61
  83.8 1.4 fusion.45
  85.2 2.4 %all_gather.7 = bf16[16,1,24,1024]{3,2,0,1:T(8,128)(2,1)S(1)} all-gather(bf16[16,1,24,512]{3,2,0,1:T(8,128)(2,1)S(1)} %fusion.45), channel_id=1, replica_groups=mesh['ep'=16,'tp'=2] {'tp'}, dimensions={3}, use_global_device_ids=true | all-gather | bytes 1179648 | tf_op jit(solution)/shard_map/all_gather | solution.py:74
  87.6 5.1 %fusion.9 = bf16[16,1,24,2048]{3,2,1,0:T(8,128)(2,1)} fusion(bf16[1,1024,2048]{2,1,0:T(8,128)(2,1)} %param.17, bf16[16,1,24,1024]{3,2,0,1:T(8,128)(2,1)S(1)} %all_gather.7), kind=kOutput, calls=%fused_computation.9 | convolution fusion | flops 1611399168 | bytes 6553600 | tf_op jit(solution)/shard_map/sjcf,jfd->sjcd/dot_general | solution.py:77
  92.7 6.4 %all-to-all-start.1 = ((bf16[16,1,24,2048]{3,2,1,0:T(8,128)(2,1)}), bf16[16,1,24,2048]{3,2,1,0:T(8,128)(2,1)S(1)}, u32[]{:S(2)}, u32[]{:S(2)}) async-start(bf16[16,1,24,2048]{3,2,1,0:T(8,128)(2,1)} %fusion.9), calls=%async_computation.5 | async-start | bytes 3145728 | tf_op jit(solution)/shard_map/all_to_all | solution.py:80
  99.2 3.6 %fusion.36 = bf16[1,1,32,1024]{3,2,1,0:T(8,128)(2,1)} fusion(bf16[32,2048]{1,0:T(8,128)(2,1)S(1)} %fusion.49, bf16[2048,1024]{1,0:T(8,128)(2,1)} %param.19), kind=kOutput, calls=%fused_computation.22 | convolution fusion | flops 134250496 | bytes 4390912 | tf_op jit(solution)/shard_map/dot_general | solution.py:54
  102.9 3.6 %fusion.35 = bf16[1,1,32,1024]{3,2,1,0:T(8,128)(2,1)} fusion(bf16[32,2048]{1,0:T(8,128)(2,1)S(1)} %fusion.49, bf16[2048,1024]{1,0:T(8,128)(2,1)} %param.18), kind=kOutput, calls=%fused_computation.21 | convolution fusion | flops 134250496 | bytes 4390912 | tf_op jit(solution)/shard_map/dot_general | solution.py:51
  106.6 5.5 %reduce-scatter.7.cloned.1.call-done = bf16[1,1,32,512]{3,2,1,0:T(8,128)(2,1)} async-done(((bf16[1,1,32,1024]{3,2,1,0:T(8,128)(2,1)}), bf16[1,1,32,512]{3,2,1,0:T(8,128)(2,1)}) %reduce-scatter.7.cloned.1.call-update) | async-done | bytes 32784 | tf_op jit(solution)/shard_map/reduce_scatter | solution.py:67
  112.1 10.7 %reduce-scatter.5.cloned.1.call-done = bf16[1,1,32,512]{3,2,1,0:T(8,128)(2,1)} async-done(((bf16[1,1,32,1024]{3,2,1,0:T(8,128)(2,1)}), bf16[1,1,32,512]{3,2,1,0:T(8,128)(2,1)}) %reduce-scatter.5.cloned.1.call-update) | async-done | bytes 32784 | tf_op jit(solution)/shard_map/reduce_scatter | solution.py:64
  122.9 0.8 fusion.56
  123.7 2.0 %all_gather.6 = bf16[1,1,32,1024]{3,2,1,0:T(8,128)(2,1)S(1)} all-gather(bf16[1,1,32,512]{3,2,1,0:T(8,128)(2,1)S(1)} %fusion.56), channel_id=1, replica_groups=mesh['ep'=16,'tp'=2] {'tp'}, dimensions={3}, use_global_device_ids=true | all-gather | bytes 98304 | tf_op jit(solution)/shard_map/all_gather | solution.py:75
  125.7 10.2 %all-to-all-done.1 = bf16[16,1,24,2048]{3,2,1,0:T(8,128)(2,1)S(1)} async-done(((bf16[16,1,24,2048]{3,2,1,0:T(8,128)(2,1)}), bf16[16,1,24,2048]{3,2,1,0:T(8,128)(2,1)S(1)}, u32[]{:S(2)}, u32[]{:S(2)}) %all-to-all-start.1) | async-done | bytes 1572896 | tf_op jit(solution)/shard_map/all_to_all | solution.py:80
  135.9 1.4 gather_fusion
  137.3 1.0 fusion.12
  138.3 3.1 %multiply_reduce_fusion = (f32[32]{0:T(128)S(1)}, f32[32,2048]{1,0:T(8,128)S(1)}) fusion(f32[32,2048]{1,0:T(8,128)S(1)} %fusion.12, bf16[1024,2048]{1,0:T(8,128)(2,1)} %param.20, bf16[1,1,32,1024]{3,2,1,0:T(8,128)(2,1)S(1)} %all_gather.6), kind=kOutput, calls=%fused_computation.41 | convolution fusion | flops 134414304 | bytes 4784256 | tf_op jit(solution)/shard_map/dot_general | solution.py:84
  141.4 3.4 %psum.15 = f32[32]{0:T(128)S(1)} all-reduce(f32[32]{0:T(128)S(1)} %get-tuple-element.5), channel_id=1, replica_groups=mesh['ep'=16,'tp'=2] {'tp'}, use_global_device_ids=true, to_apply=%region_10.11 | all-reduce | flops 32 | bytes 256 | tf_op jit(solution)/shard_map/psum | solution.py:88
  (24 shorter events, 2.9 us)
Async XLA Ops:
  6.5 65.7 %reduce-scatter.9.cloned.1.call-start = ((), (), s32[]{:S(2)}) async-start(), calls=%async_computation.8 | async-start | bytes 1179648 | tf_op jit(solution)/shard_map/reduce_scatter | solution.py:58
  63.1 20.7 %reduce-scatter.11.cloned.1.call-start = ((), (), s32[]{:S(2)}) async-start(), calls=%async_computation.9 | async-start | bytes 1179648 | tf_op jit(solution)/shard_map/reduce_scatter | solution.py:61
  92.7 43.2 %all-to-all-start.1 = ((bf16[16,1,24,2048]{3,2,1,0:T(8,128)(2,1)}), bf16[16,1,24,2048]{3,2,1,0:T(8,128)(2,1)S(1)}, u32[]{:S(2)}, u32[]{:S(2)}) async-start(bf16[16,1,24,2048]{3,2,1,0:T(8,128)(2,1)} %fusion.9), calls=%async_computation.5 | async-start | bytes 3145728 | tf_op jit(solution)/shard_map/all_to_all | solution.py:80
  99.1 7.4 %copy-start.1 = (f32[32,8]{0,1:T(8,128)S(1)}, f32[32,8]{0,1:T(8,128)}, u32[]{:S(2)}) copy-start(f32[32,8]{0,1:T(8,128)} %param.14) | copy-start | bytes 3076
  99.1 13.0 %reduce-scatter.7.cloned.1.call-start = ((), (), s32[]{:S(2)}) async-start(), calls=%async_computation.7 | async-start | bytes 98304 | tf_op jit(solution)/shard_map/reduce_scatter | solution.py:67
  102.8 20.1 %reduce-scatter.5.cloned.1.call-start = ((), (), s32[]{:S(2)}) async-start(), calls=%async_computation.6 | async-start | bytes 98304 | tf_op jit(solution)/shard_map/reduce_scatter | solution.py:64
  137.3 7.5 %copy-start = (f32[2048]{0:T(1024)S(1)}, f32[2048]{0:T(1024)}, u32[]{:S(2)}) copy-start(f32[2048]{0:T(1024)} %param.21) | copy-start | bytes 24580
Sparse Core Ops, SparseCore 0:
  63.3 8.9 reduce-scatter.8
  74.5 9.2 reduce-scatter.10
  103.0 9.1 reduce-scatter.6
  114.2 8.6 reduce-scatter.4
where the time goes:
time: 153 us; the launch traced here: 152 us
  blocking collectives  53 us (35%)
  waiting for transfers between devices  42.2 us (28%)
  matrix products  25.3 us (17%)
  between operations  13.2 us (9%)
  other arithmetic  6.83 us (4%)
  starting transfers between devices  6.53 us (4%)
  local copies, waits for them, and re-layouts  5.07 us (3%)
    all_to_all x1, blocking collectives, per_device(): lax.all_to_all(outgoing, 'ep', split_axis=0, concat_axis=0, tiled=True)  42.3 us
    reduce_scatter x1, waiting for transfers between devices, per_device(): lax.psum_scatter(up_part.astype(jnp.bfloat16), 'tp', scatter_dimension=3,...  11.6 us
    reduce_scatter x1, waiting for transfers between devices, per_device(): lax.psum_scatter(shared_gate_part.astype(jnp.bfloat16), 'tp', scatter_dim...  10.7 us
    all_to_all x1, waiting for transfers between devices, per_device(): lax.all_to_all(expert_rows, 'ep', split_axis=0, concat_axis=0, tiled=True)  10.2 us
    all_to_all x1, starting transfers between devices, per_device(): lax.all_to_all(expert_rows, 'ep', split_axis=0, concat_axis=0, tiled=True)  6.41 us
    reduce_scatter x1, waiting for transfers between devices, per_device(): lax.psum_scatter(shared_up_part.astype(jnp.bfloat16), 'tp', scatter_dimen...  5.51 us
    dot_general x1, matrix products, per_device(): jnp.einsum('sjcf,jfd->sjcd', hidden, down_proj, preferred_element_type=jn...  5.14 us
    dot_general x1, matrix products, per_device(): jnp.einsum('sjcd,jdf->sjcf', arrived, up_proj, preferred_element_type=jnp...  4.89 us
  transfers between devices with their start and end apart: 5, of which 5 were waited for; matrix products, arithmetic and copies ran while one was open for 9% of the time, Pallas kernels for 0%

commit v1 on v0

--- a/solution.py
+++ b/solution.py
@@ -1,9 +1,419 @@
+import functools
+
 import jax
 import jax.numpy as jnp
 from jax import lax
+from jax.experimental import pallas as pl
+from jax.experimental.pallas import tpu as pltpu
 from jax.sharding import PartitionSpec as P
 
-D = 4096
+
+F32 = jnp.float32
+BF16 = jnp.bfloat16
+
+
+def layer_kernel(
+    zs,
+    tokens_ref,
+    gain_ref,
+    routes_ref,
+    rw_ref,
+    out_gain_ref,
+    gate_hbm,
+    up_hbm,
+    down_hbm,
+    sgate_hbm,
+    sup_hbm,
+    sdown_hbm,
+    out_ref,
+    wg,
+    wu,
+    wd,
+    sg,
+    su,
+    sd,
+    slab,
+    gu_s,
+    gu_r,
+    sh_s,
+    sh_r,
+    ss_s,
+    ss_r,
+    sbuf,
+    rbuf,
+    sz,
+    rz,
+    acc_x,
+    acc_y,
+    acc_o,
+    obuf,
+    shared_out,
+    hid,
+    w_sem,
+    ag_send,
+    ag_recv,
+    rs_send,
+    rs_recv,
+    z_send,
+    z_recv,
+    ex_send,
+    ex_recv,
+):
+    rows, dl = tokens_ref.shape
+    d_all = dl * 2
+    half = dl // 2
+    f = wg.shape[1]
+    fs = sg.shape[1]
+    chunk = zs * rows
+    experts = zs * 4
+    wide = slab.shape[3]
+
+    me = lax.axis_index("ep")
+    tp = lax.axis_index("tp")
+    x, y, z = lax.rem(me, 2), lax.rem(me // 2, 2), me // 4
+    own = y * 2 + x
+    xcol = y * 2 + (1 - x)
+    ycol = (1 - y) * 2 + x
+    dcol = (1 - y) * 2 + (1 - x)
+    x_dev = z * 4 + xcol
+    y_dev = z * 4 + ycol
+    zlist = [lax.rem(z + dz, zs) for dz in range(zs)]
+    zdevs = [zi * 4 + own for zi in zlist]
+
+    def ep_dev(e):
+        return (e, tp)
+
+    peer = (me, 1 - tp)
+    pending = []
+
+    def send(src, dst, ssem, rsem, dev):
+        c = pltpu.make_async_remote_copy(
+            src_ref=src,
+            dst_ref=dst,
+            send_sem=ssem,
+            recv_sem=rsem,
+            device_id=dev,
+            device_id_type=pl.DeviceIdType.MESH,
+        )
+        c.start()
+        pending.append(c)
+
+    def landed(ref, rsem):
+        pltpu.make_async_remote_copy(
+            src_ref=ref,
+            dst_ref=ref,
+            send_sem=rsem,
+            recv_sem=rsem,
+            device_id=peer,
+            device_id_type=pl.DeviceIdType.MESH,
+        ).wait_recv()
+
+    loads = []
+    for i, (src, dst) in enumerate(
+        (
+            (sgate_hbm, sg),
+            (sup_hbm, su),
+            (gate_hbm.at[0], wg),
+            (up_hbm.at[0], wu),
+            (sdown_hbm, sd),
+            (down_hbm.at[0], wd),
+        )
+    ):
+        c = pltpu.make_async_copy(src, dst, w_sem.at[i])
+        c.start()
+        loads.append(c)
+
+    barrier = pltpu.get_barrier_semaphore()
+    others = [peer, ep_dev(x_dev), ep_dev(y_dev)] + [ep_dev(e) for e in zdevs[1:]]
+    for dev in others:
+        pl.semaphore_signal(barrier, inc=1, device_id=dev, device_id_type=pl.DeviceIdType.MESH)
+
+    tok = tokens_ref[...].astype(F32)
+    squares = jnp.sum(tok * tok, axis=1, keepdims=True)
+    ss_s[0] = jnp.broadcast_to(squares, (rows, 128))
+    lanes = lax.broadcasted_iota(jnp.int32, (rows, wide - dl), 1)
+    wmat = jnp.zeros((rows, wide - dl), F32)
+    wlow = jnp.zeros((rows, wide - dl), F32)
+    for k in range(routes_ref.shape[1]):
+        pick = routes_ref[:, k : k + 1]
+        val = rw_ref[:, k : k + 1]
+        high = val.astype(BF16).astype(F32)
+        wmat = wmat + jnp.where(lanes == pick, high, 0.0)
+        wlow = wlow + jnp.where(lanes == pick + experts, val - high, 0.0)
+    slab[own, z, :, dl:wide] = (wmat + wlow).astype(BF16)
+
+    pl.semaphore_wait(barrier, len(others))
+    send(ss_s.at[0], ss_r.at[0], ex_send.at[0], ex_recv.at[0], peer)
+    landed(ss_r.at[0], ex_recv.at[0])
+    total = squares + ss_r[0][:, 0:1]
+    normed = (tok * lax.rsqrt(total / d_all + 1e-06) * gain_ref[...]).astype(BF16)
+    slab[own, z, :, 0:dl] = normed
+
+    mine = slab.at[own, z]
+    for dz in range(1, zs):
+        send(mine, mine, ag_send.at[0, dz], ag_recv.at[0, z], ep_dev(zdevs[dz]))
+    send(mine, mine, ag_send.at[1, 0], ag_recv.at[1, z], ep_dev(x_dev))
+    send(mine, mine, ag_send.at[2, 0], ag_recv.at[2, z], ep_dev(y_dev))
+
+    def relay_own(dz):
+        zi = zlist[dz]
+        ref = slab.at[own, zi]
+        landed(ref, ag_recv.at[0, zi])
+        send(ref, ref, ag_send.at[1, dz], ag_recv.at[1, zi], ep_dev(x_dev))
+        send(ref, ref, ag_send.at[2, dz], ag_recv.at[2, zi], ep_dev(y_dev))
+
+    low, high_part = pl.ds(0, half), pl.ds(half, wide - half)
+
+    def relay_side(dz):
+        zi = zlist[dz]
+        landed(slab.at[xcol, zi], ag_recv.at[1, zi])
+        ref = slab.at[xcol, zi, :, low]
+        send(ref, ref, ag_send.at[3, dz], ag_recv.at[3, zi], ep_dev(y_dev))
+        landed(slab.at[ycol, zi], ag_recv.at[2, zi])
+        ref = slab.at[ycol, zi, :, high_part]
+        send(ref, ref, ag_send.at[4, dz], ag_recv.at[4, zi], ep_dev(x_dev))
+
+    def silu_mul(g, u):
+        return (g / (1.0 + jnp.exp(-g)) * u).astype(BF16)
+
+    loads[0].wait()
+    loads[1].wait()
+    tile = 256
+
+    def shared_step(j, carry):
+        cols = pl.ds(pl.multiple_of(j * tile, tile), tile)
+        cols_up = pl.ds(pl.multiple_of(fs + j * tile, tile), tile)
+        v = slab[own, z, :, 0:dl]
+        sh_s[:, cols] = jnp.dot(v, sg[:, cols], preferred_element_type=F32).astype(BF16)
+        sh_s[:, cols_up] = jnp.dot(v, su[:, cols], preferred_element_type=F32).astype(BF16)
+        return carry
+
+    lax.fori_loop(0, fs // tile, shared_step, 0)
+    send(sh_s, sh_r, ex_send.at[1], ex_recv.at[1], peer)
+
+    relay_own(1) if zs > 1 else None
+    relay_side(0)
+
+    landed(sh_r, ex_recv.at[1])
+    loads[4].wait()
+    sg_pre = sh_s[:, 0:fs].astype(F32) + sh_r[:, 0:fs].astype(F32)
+    su_pre = sh_s[:, fs : 2 * fs].astype(F32) + sh_r[:, fs : 2 * fs].astype(F32)
+    sh_hid = silu_mul(sg_pre, su_pre)
+    for j in range(0, dl, 512):
+        shared_out[:, j : j + 512] = jnp.dot(
+            sh_hid, sd[:, j : j + 512], preferred_element_type=F32
+        )
+
+    for dz in range(2, zs):
+        relay_own(dz)
+        relay_side(dz - 1)
+
+    loads[2].wait()
+    loads[3].wait()
+
+    def first(col, i):
+        def step(j, carry):
+            cols = pl.ds(pl.multiple_of(j * tile, tile), tile)
+            cols_up = pl.ds(pl.multiple_of(f + j * tile, tile), tile)
+            v = slab[col, :, :, 0:dl].reshape(chunk, dl)
+            gu_s[i, :, cols] = jnp.dot(v, wg[:, cols], preferred_element_type=F32).astype(BF16)
+            gu_s[i, :, cols_up] = jnp.dot(v, wu[:, cols], preferred_element_type=F32).astype(BF16)
+            return carry
+
+        lax.fori_loop(0, f // tile, step, 0)
+        send(gu_s.at[i], gu_r.at[i], ex_send.at[2 + i], ex_recv.at[2 + i], peer)
+
+    def second(col, i):
+        landed(gu_r.at[i], ex_recv.at[2 + i])
+
+        def act(j, carry):
+            cols = pl.ds(pl.multiple_of(j * tile, tile), tile)
+            cols_up = pl.ds(pl.multiple_of(f + j * tile, tile), tile)
+            g = gu_s[i, :, cols].astype(F32) + gu_r[i, :, cols].astype(F32)
+            u = gu_s[i, :, cols_up].astype(F32) + gu_r[i, :, cols_up].astype(F32)
+            hid[:, cols] = silu_mul(g, u)
+            return carry
+
+        lax.fori_loop(0, f // tile, act, 0)
+        wcols = slab[col, :, :, dl:wide].reshape(chunk, wide - dl).astype(F32)
+        spots = lax.broadcasted_iota(jnp.int32, wcols.shape, 1)
+        chosen = (spots == me) | (spots == me + experts)
+        weight = jnp.sum(jnp.where(chosen, wcols, 0.0), axis=1, keepdims=True)
+
+        def down(j, carry):
+            cols = pl.ds(pl.multiple_of(j * tile, tile), tile)
+            out = jnp.dot(hid[...], wd[:, cols], preferred_element_type=F32)
+            obuf[:, cols] = out.astype(BF16).astype(F32) * weight
+            return carry
+
+        lax.fori_loop(0, dl // tile, down, 0)
+
+    def shaped(v):
+        return v.astype(BF16).reshape(zs, rows, half)
+
+    X1, Y1, DA, DB, X2, Y2 = range(6)
+
+    def rs(kind, dz, dev):
+        zi = zlist[dz]
+        send(
+            sbuf.at[kind, zi], rbuf.at[kind, zi], rs_send.at[kind, zi], rs_recv.at[kind, zi], dev
+        )
+
+    def rs_landed(kind, dz):
+        zi = zlist[dz]
+        landed(rbuf.at[kind, zi], rs_recv.at[kind, zi])
+        return rbuf[kind, zi].astype(F32)
+
+    order = list(range(1, zs)) + [0]
+
+    first(own, 0)
+    relay_side(zs - 1) if zs > 1 else None
+    loads[5].wait()
+    second(own, 0)
+    acc_o[...] = obuf[...].reshape(zs, rows, dl)
+    first(xcol, 1)
+    first(ycol, 2)
+    second(xcol, 1)
+    sbuf[X1] = shaped(obuf[:, half:dl])
+    for dz in order:
+        rs(X1, dz, ep_dev(x_dev))
+    acc_x[...] = obuf[:, 0:half].reshape(zs, rows, half)
+    second(ycol, 2)
+    sbuf[Y1] = shaped(obuf[:, 0:half])
+    for dz in order:
+        rs(Y1, dz, ep_dev(y_dev))
+    acc_y[...] = obuf[:, half:dl].reshape(zs, rows, half)
+    for dz in range(zs):
+        zi = zlist[dz]
+        landed(slab.at[dcol, zi, :, low], ag_recv.at[3, zi])
+        landed(slab.at[dcol, zi, :, high_part], ag_recv.at[4, zi])
+    first(dcol, 3)
+    second(dcol, 3)
+    sbuf[DA] = shaped(obuf[:, 0:half])
+    sbuf[DB] = shaped(obuf[:, half:dl])
+    for dz in order:
+        rs(DA, dz, ep_dev(y_dev))
+        rs(DB, dz, ep_dev(x_dev))
+
+    def middle(dz):
+        zi = zlist[dz]
+        sbuf[X2, zi] = (acc_x[zi] + rs_landed(DA, dz)).astype(BF16)
+        rs(X2, dz, ep_dev(x_dev))
+        sbuf[Y2, zi] = (acc_y[zi] + rs_landed(DB, dz)).astype(BF16)
+        rs(Y2, dz, ep_dev(y_dev))
+
+    def last(dz):
+        zi = zlist[dz]
+        left = acc_o[zi, :, 0:half] + rs_landed(Y1, dz) + rs_landed(X2, dz)
+        right = acc_o[zi, :, half:dl] + rs_landed(X1, dz) + rs_landed(Y2, dz)
+        if dz == 0:
+            acc_o[zi, :, 0:half] = left
+            acc_o[zi, :, half:dl] = right
+        else:
+            sz[dz, :, 0:half] = left.astype(BF16)
+            sz[dz, :, half:dl] = right.astype(BF16)
+            send(sz.at[dz], rz.at[z], z_send.at[dz], z_recv.at[z], ep_dev(zdevs[dz]))
+
+    for n, dz in enumerate(order):
+        middle(dz)
+        if n > 0:
+            last(order[n - 1])
+    last(order[-1])
+
+    mixed = shared_out[...] + acc_o[z]
+    for dz in range(1, zs):
+        zi = zlist[dz]
+        landed(rz.at[zi], z_recv.at[zi])
+        mixed = mixed + rz[zi].astype(F32)
+    final = jnp.sum(mixed * mixed, axis=1, keepdims=True)
+    ss_s[1] = jnp.broadcast_to(final, (rows, 128))
+    send(ss_s.at[1], ss_r.at[1], ex_send.at[6], ex_recv.at[6], peer)
+    landed(ss_r.at[1], ex_recv.at[6])
+    final = final + ss_r[1][:, 0:1]
+    out_ref[...] = (mixed * lax.rsqrt(final / d_all + 1e-06) * out_gain_ref[...]).astype(BF16)
+    for c in pending:
+        c.wait_send()
+
+
+def fused(
+    tokens,
+    norm_gain,
+    routes,
+    route_weights,
+    gate_proj,
+    up_proj,
+    down_proj,
+    shared_gate,
+    shared_up,
+    shared_down,
+    out_gain,
+):
+    rows, dl = tokens.shape
+    ep = lax.axis_size("ep")
+    zs = ep // 4
+    f = gate_proj.shape[2]
+    fs = shared_gate.shape[1]
+    half = dl // 2
+    chunk = zs * rows
+    wide = dl + -(-2 * ep // 128) * 128
+    vmem = pl.BlockSpec(memory_space=pltpu.VMEM)
+    anys = pl.BlockSpec(memory_space=pl.ANY)
+    dma = pltpu.SemaphoreType.DMA
+    return pl.pallas_call(
+        functools.partial(layer_kernel, zs),
+        out_shape=jax.ShapeDtypeStruct((rows, dl), BF16),
+        in_specs=[vmem] * 5 + [anys] * 6,
+        out_specs=vmem,
+        scratch_shapes=[
+            pltpu.VMEM((dl, f), BF16),
+            pltpu.VMEM((dl, f), BF16),
+            pltpu.VMEM((f, dl), BF16),
+            pltpu.VMEM((dl, fs), BF16),
+            pltpu.VMEM((dl, fs), BF16),
+            pltpu.VMEM((fs, dl), BF16),
+            pltpu.VMEM((4, zs, rows, wide), BF16),
+            pltpu.VMEM((4, chunk, 2 * f), BF16),
+            pltpu.VMEM((4, chunk, 2 * f), BF16),
+            pltpu.VMEM((rows, 2 * fs), BF16),
+            pltpu.VMEM((rows, 2 * fs), BF16),
+            pltpu.VMEM((2, rows, 128), F32),
+            pltpu.VMEM((2, rows, 128), F32),
+            pltpu.VMEM((6, zs, rows, half), BF16),
+            pltpu.VMEM((6, zs, rows, half), BF16),
+            pltpu.VMEM((zs, rows, dl), BF16),
+            pltpu.VMEM((zs, rows, dl), BF16),
+            pltpu.VMEM((zs, rows, half), F32),
+            pltpu.VMEM((zs, rows, half), F32),
+            pltpu.VMEM((zs, rows, dl), F32),
+            pltpu.VMEM((chunk, dl), F32),
+            pltpu.VMEM((rows, dl), F32),
+            pltpu.VMEM((chunk, f), BF16),
+            dma((6,)),
+            dma((5, zs)),
+            dma((5, zs)),
+            dma((6, zs)),
+            dma((6, zs)),
+            dma((zs,)),
+            dma((zs,)),
+            dma((7,)),
+            dma((7,)),
+        ],
+        compiler_params=pltpu.CompilerParams(
+            collective_id=0, has_side_effects=True, vmem_limit_bytes=60 * 1024 * 1024
+        ),
+    )(
+        tokens,
+        norm_gain.reshape(1, dl),
+        routes,
+        route_weights,
+        out_gain.reshape(1, dl),
+        gate_proj,
+        up_proj,
+        down_proj,
+        shared_gate,
+        shared_up,
+        shared_down,
+    )
 
 
 def per_device(
@@ -19,9 +429,10 @@
     shared_down,
     out_gain,
 ):
+    features = tokens.shape[1] * lax.axis_size("tp")
     tokens_f = tokens.astype(jnp.float32)
     squares = lax.psum(jnp.sum(tokens_f * tokens_f, axis=1), "tp")
-    normed = (tokens_f * lax.rsqrt(squares / D + 1e-06)[:, None] * norm_gain[None, :]).astype(
+    normed = (tokens_f * lax.rsqrt(squares / features + 1e-06)[:, None] * norm_gain[None, :]).astype(
         jnp.bfloat16
     )
     tok_rows, picks = routes.shape
@@ -86,14 +497,20 @@
     )
     mixed = shared_part + routed
     final_squares = lax.psum(jnp.sum(mixed * mixed, axis=1), "tp")
-    return (mixed * lax.rsqrt(final_squares / D + 1e-06)[:, None] * out_gain[None, :]).astype(
+    return (mixed * lax.rsqrt(final_squares / features + 1e-06)[:, None] * out_gain[None, :]).astype(
         jnp.bfloat16
     )
 
 
 def solution(mesh):
+    one_chip_pair = mesh.shape["tp"] == 2 and mesh.shape["ep"] % 4 == 0
+
+    def step(*args):
+        fits = one_chip_pair and args[4].shape[0] == 1
+        return (fused if fits else per_device)(*args)
+
     return jax.shard_map(
-        per_device,
+        step,
         mesh=mesh,
         in_specs=(
             P("ep", "tp"),

time: 153 us -> 79.4 us (0.52)
  Pallas kernels: 0 us -> 74.4 us
  blocking collectives: 53 us -> 0 us
  waiting for transfers between devices: 42.2 us -> 0 us
  matrix products: 25.3 us -> 0 us
  between operations: 13.2 us -> 0.01 us
  other arithmetic: 6.83 us -> 0 us
  starting transfers between devices: 6.53 us -> 0 us
    pallas_call x0 -> x1, Pallas kernels: none -> 74.4 us  [fused(): pl.pallas_call(functools.partial(layer_kernel, zs), out_shape=jax.ShapeDt...]
    all_to_all x1 -> x0, blocking collectives: 42.3 us -> none  [per_device(): lax.all_to_all(outgoing, 'ep', split_axis=0, concat_axis=0, tiled=True)]
    reduce_scatter x4 -> x0, waiting for transfers between devices: 32 us -> none  [the longest x1 11.6 us: per_device(): lax.psum_scatter(up_part.astype(jnp.bfloat16), 'tp', scatter_dimension=3,...]
    dot_general x6 -> x0, matrix products: 25.3 us -> none  [the longest x1 5.14 us: per_device(): jnp.einsum('sjcf,jfd->sjcd', hidden, down_proj, preferred_element_type=jn...]
    all_to_all x1 -> x0, waiting for transfers between devices: 10.2 us -> none  [per_device(): lax.all_to_all(expert_rows, 'ep', split_axis=0, concat_axis=0, tiled=True)]
    all_to_all x1 -> x0, starting transfers between devices: 6.41 us -> none  [per_device(): lax.all_to_all(expert_rows, 'ep', split_axis=0, concat_axis=0, tiled=True)]
    psum x2 -> x0, blocking collectives: 6.23 us -> none  [the longest x1 3.43 us: per_device(): final_squares = lax.psum(jnp.sum(mixed * mixed, axis=1), 'tp')]
    all_gather x2 -> x0, blocking collectives: 4.4 us -> none  [the longest x1 2.37 us: per_device(): lax.all_gather(hidden_piece, 'tp', axis=3, tiled=True)]
  transfers between devices with their start and end apart: 5 -> 0, of which waited for: 5 -> 0; matrix products, arithmetic and copies ran while one was open for 9% -> 0% of each run, Pallas kernels for 0% -> 0%
where the time goes in v1:
time: 79.4 us; the launch traced here: 78.7 us
  Pallas kernels  74.4 us (94%)
  local copies, waits for them, and re-layouts  4.29 us (5%)
    pallas_call x1, Pallas kernels, fused(): pl.pallas_call(functools.partial(layer_kernel, zs), out_shape=jax.ShapeDt...  74.4 us
    unnamed x3, local copies, waits for them, and re-layouts  4.29 us

profile of v1, /device:TPU:13, one launch (start us, length us, event | category | flops | bytes accessed | tf_op | source)
XLA Modules:
  0.0 78.7 jit_solution(17865094204135990531)
XLA Ops:
  0.0 1.4 %copy.12.routes_ref = s32[32,8]{1,0:T(8,128)} copy(s32[32,8]{0,1:T(8,128)} %param.13) | data formatting | bytes 2048 | tf_op args[2]
  1.4 1.4 %copy.13.rw_ref = f32[32,8]{1,0:T(8,128)} copy(f32[32,8]{0,1:T(8,128)} %param.14) | data formatting | bytes 2048 | tf_op args[3]
  2.7 74.4 %shard_map.109 = bf16[32,2048]{1,0:T(8,128)(2,1)} custom-call(bf16[32,2048]{1,0:T(8,128)(2,1)} %tokens_ref.1, f32[1,2048]{1,0:T(1,128)} %bitcast.2, s32[32,8]{1,0:T(8,128)} %copy.12.routes_ref, f32[32,8]{1,0:T(8,128)} %copy.13.rw_ref, f32[1,2048]{1,0:T(1,128)} %bitcast.3, bf16[1,2048,1024]{2,1,0:T(8,128)(2,1)} %gate_hbm.1, bf16[1,2048,1024]{2,1,0:T(8,128)(2,1)} %up_hbm.1, ...), custom_call_target="tpu_custom_call" | custom-call | tf_op jit(solution)/shard_map/pallas_call | solution.py:362
  77.2 1.6 %copy.15 = bf16[32,2048]{1,0:T(8,128)(2,1)} copy(bf16[32,2048]{1,0:T(8,128)(2,1)} %shard_map.109) | data formatting | bytes 262144

commit v2 on v1

--- a/solution.py
+++ b/solution.py
@@ -77,7 +77,7 @@
     dcol = (1 - y) * 2 + (1 - x)
     x_dev = z * 4 + xcol
     y_dev = z * 4 + ycol
-    zlist = [lax.rem(z + dz, zs) for dz in range(zs)]
+    zlist = [lax.rem(z + zs - dz, zs) for dz in range(zs)]
     zdevs = [zi * 4 + own for zi in zlist]
 
     def ep_dev(e):
@@ -131,16 +131,25 @@
     tok = tokens_ref[...].astype(F32)
     squares = jnp.sum(tok * tok, axis=1, keepdims=True)
     ss_s[0] = jnp.broadcast_to(squares, (rows, 128))
-    lanes = lax.broadcasted_iota(jnp.int32, (rows, wide - dl), 1)
-    wmat = jnp.zeros((rows, wide - dl), F32)
-    wlow = jnp.zeros((rows, wide - dl), F32)
-    for k in range(routes_ref.shape[1]):
-        pick = routes_ref[:, k : k + 1]
-        val = rw_ref[:, k : k + 1]
-        high = val.astype(BF16).astype(F32)
-        wmat = wmat + jnp.where(lanes == pick, high, 0.0)
-        wlow = wlow + jnp.where(lanes == pick + experts, val - high, 0.0)
-    slab[own, z, :, dl:wide] = (wmat + wlow).astype(BF16)
+    spread = (wide - dl, rows)
+    names = lax.broadcasted_iota(jnp.int32, spread, 0)
+    wmat = jnp.zeros(spread, F32)
+    for k in range(routes_ref.shape[0]):
+        pick = routes_ref[k : k + 1, :]
+        val = rw_ref[k : k + 1, :]
+        upper = val.astype(BF16).astype(F32)
+        wmat = wmat + jnp.where(names == pick, upper, 0.0)
+        wmat = wmat + jnp.where(names == pick + experts, val - upper, 0.0)
+    square = (rows, rows)
+    eye = (
+        lax.broadcasted_iota(jnp.int32, square, 0) == lax.broadcasted_iota(jnp.int32, square, 1)
+    ).astype(F32)
+    slab[own, z, :, dl:wide] = lax.dot_general(
+        eye.astype(BF16),
+        wmat.astype(BF16),
+        (((1,), (1,)), ((), ())),
+        preferred_element_type=F32,
+    ).astype(BF16)
 
     pl.semaphore_wait(barrier, len(others))
     send(ss_s.at[0], ss_r.at[0], ex_send.at[0], ex_recv.at[0], peer)
@@ -151,7 +160,7 @@
 
     mine = slab.at[own, z]
     for dz in range(1, zs):
-        send(mine, mine, ag_send.at[0, dz], ag_recv.at[0, z], ep_dev(zdevs[dz]))
+        send(mine, mine, ag_send.at[0, dz], ag_recv.at[0, z], ep_dev(zdevs[zs - dz]))
     send(mine, mine, ag_send.at[1, 0], ag_recv.at[1, z], ep_dev(x_dev))
     send(mine, mine, ag_send.at[2, 0], ag_recv.at[2, z], ep_dev(y_dev))
 
@@ -194,16 +203,6 @@
     relay_own(1) if zs > 1 else None
     relay_side(0)
 
-    landed(sh_r, ex_recv.at[1])
-    loads[4].wait()
-    sg_pre = sh_s[:, 0:fs].astype(F32) + sh_r[:, 0:fs].astype(F32)
-    su_pre = sh_s[:, fs : 2 * fs].astype(F32) + sh_r[:, fs : 2 * fs].astype(F32)
-    sh_hid = silu_mul(sg_pre, su_pre)
-    for j in range(0, dl, 512):
-        shared_out[:, j : j + 512] = jnp.dot(
-            sh_hid, sd[:, j : j + 512], preferred_element_type=F32
-        )
-
     for dz in range(2, zs):
         relay_own(dz)
         relay_side(dz - 1)
@@ -211,42 +210,36 @@
     loads[2].wait()
     loads[3].wait()
 
+    pieces = gu_s.shape[1]
+    part = f // pieces
+
     def first(col, i):
-        def step(j, carry):
-            cols = pl.ds(pl.multiple_of(j * tile, tile), tile)
-            cols_up = pl.ds(pl.multiple_of(f + j * tile, tile), tile)
+        for j in range(pieces):
+            cols = slice(j * part, (j + 1) * part)
             v = slab[col, :, :, 0:dl].reshape(chunk, dl)
-            gu_s[i, :, cols] = jnp.dot(v, wg[:, cols], preferred_element_type=F32).astype(BF16)
-            gu_s[i, :, cols_up] = jnp.dot(v, wu[:, cols], preferred_element_type=F32).astype(BF16)
-            return carry
-
-        lax.fori_loop(0, f // tile, step, 0)
-        send(gu_s.at[i], gu_r.at[i], ex_send.at[2 + i], ex_recv.at[2 + i], peer)
+            g = jnp.dot(v, wg[:, cols], preferred_element_type=F32)
+            gu_s[i, j, :, 0:part] = g.astype(BF16)
+            u = jnp.dot(v, wu[:, cols], preferred_element_type=F32)
+            gu_s[i, j, :, part : 2 * part] = u.astype(BF16)
+            n = 3 + i * pieces + j
+            send(gu_s.at[i, j], gu_r.at[i, j], ex_send.at[n], ex_recv.at[n], peer)
 
     def second(col, i):
-        landed(gu_r.at[i], ex_recv.at[2 + i])
-
-        def act(j, carry):
-            cols = pl.ds(pl.multiple_of(j * tile, tile), tile)
-            cols_up = pl.ds(pl.multiple_of(f + j * tile, tile), tile)
-            g = gu_s[i, :, cols].astype(F32) + gu_r[i, :, cols].astype(F32)
-            u = gu_s[i, :, cols_up].astype(F32) + gu_r[i, :, cols_up].astype(F32)
-            hid[:, cols] = silu_mul(g, u)
-            return carry
-
-        lax.fori_loop(0, f // tile, act, 0)
+        for j in range(pieces):
+            landed(gu_r.at[i, j], ex_recv.at[3 + i * pieces + j])
+            g = gu_s[i, j, :, 0:part].astype(F32) + gu_r[i, j, :, 0:part].astype(F32)
+            u = gu_s[i, j, :, part:].astype(F32) + gu_r[i, j, :, part:].astype(F32)
+            hid[:, j * part : (j + 1) * part] = silu_mul(g, u)
         wcols = slab[col, :, :, dl:wide].reshape(chunk, wide - dl).astype(F32)
         spots = lax.broadcasted_iota(jnp.int32, wcols.shape, 1)
         chosen = (spots == me) | (spots == me + experts)
         weight = jnp.sum(jnp.where(chosen, wcols, 0.0), axis=1, keepdims=True)
 
-        def down(j, carry):
-            cols = pl.ds(pl.multiple_of(j * tile, tile), tile)
+        step = min(512, dl)
+        for j in range(0, dl, step):
+            cols = slice(j, j + step)
             out = jnp.dot(hid[...], wd[:, cols], preferred_element_type=F32)
             obuf[:, cols] = out.astype(BF16).astype(F32) * weight
-            return carry
-
-        lax.fori_loop(0, dl // tile, down, 0)
 
     def shaped(v):
         return v.astype(BF16).reshape(zs, rows, half)
@@ -269,8 +262,6 @@
     first(own, 0)
     relay_side(zs - 1) if zs > 1 else None
     loads[5].wait()
-    second(own, 0)
-    acc_o[...] = obuf[...].reshape(zs, rows, dl)
     first(xcol, 1)
     first(ycol, 2)
     second(xcol, 1)
@@ -295,6 +286,18 @@
         rs(DA, dz, ep_dev(y_dev))
         rs(DB, dz, ep_dev(x_dev))
 
+    second(own, 0)
+    acc_o[...] = obuf[...].reshape(zs, rows, dl)
+    landed(sh_r, ex_recv.at[1])
+    loads[4].wait()
+    sg_pre = sh_s[:, 0:fs].astype(F32) + sh_r[:, 0:fs].astype(F32)
+    su_pre = sh_s[:, fs : 2 * fs].astype(F32) + sh_r[:, fs : 2 * fs].astype(F32)
+    sh_hid = silu_mul(sg_pre, su_pre)
+    for j in range(0, dl, 512):
+        shared_out[:, j : j + 512] = jnp.dot(
+            sh_hid, sd[:, j : j + 512], preferred_element_type=F32
+        )
+
     def middle(dz):
         zi = zlist[dz]
         sbuf[X2, zi] = (acc_x[zi] + rs_landed(DA, dz)).astype(BF16)
@@ -327,8 +330,8 @@
         mixed = mixed + rz[zi].astype(F32)
     final = jnp.sum(mixed * mixed, axis=1, keepdims=True)
     ss_s[1] = jnp.broadcast_to(final, (rows, 128))
-    send(ss_s.at[1], ss_r.at[1], ex_send.at[6], ex_recv.at[6], peer)
-    landed(ss_r.at[1], ex_recv.at[6])
+    send(ss_s.at[1], ss_r.at[1], ex_send.at[2], ex_recv.at[2], peer)
+    landed(ss_r.at[1], ex_recv.at[2])
     final = final + ss_r[1][:, 0:1]
     out_ref[...] = (mixed * lax.rsqrt(final / d_all + 1e-06) * out_gain_ref[...]).astype(BF16)
     for c in pending:
@@ -356,6 +359,7 @@
     half = dl // 2
     chunk = zs * rows
     wide = dl + -(-2 * ep // 128) * 128
+    pieces = max(1, f // 512)
     vmem = pl.BlockSpec(memory_space=pltpu.VMEM)
     anys = pl.BlockSpec(memory_space=pl.ANY)
     dma = pltpu.SemaphoreType.DMA
@@ -372,8 +376,8 @@
             pltpu.VMEM((dl, fs), BF16),
             pltpu.VMEM((fs, dl), BF16),
             pltpu.VMEM((4, zs, rows, wide), BF16),
-            pltpu.VMEM((4, chunk, 2 * f), BF16),
-            pltpu.VMEM((4, chunk, 2 * f), BF16),
+            pltpu.VMEM((4, pieces, chunk, 2 * f // pieces), BF16),
+            pltpu.VMEM((4, pieces, chunk, 2 * f // pieces), BF16),
             pltpu.VMEM((rows, 2 * fs), BF16),
             pltpu.VMEM((rows, 2 * fs), BF16),
             pltpu.VMEM((2, rows, 128), F32),
@@ -395,8 +399,8 @@
             dma((6, zs)),
             dma((zs,)),
             dma((zs,)),
-            dma((7,)),
-            dma((7,)),
+            dma((3 + 4 * pieces,)),
+            dma((3 + 4 * pieces,)),
         ],
         compiler_params=pltpu.CompilerParams(
             collective_id=0, has_side_effects=True, vmem_limit_bytes=60 * 1024 * 1024
@@ -404,8 +408,8 @@
     )(
         tokens,
         norm_gain.reshape(1, dl),
-        routes,
-        route_weights,
+        routes.T,
+        route_weights.T,
         out_gain.reshape(1, dl),
         gate_proj,
         up_proj,

time: 79.4 us -> 66.8 us (0.84)
  the two profiles are of different devices: /device:TPU:13 before, /device:TPU:1 now
where the time goes in v2:
time: 66.8 us; the launch traced here: 66.6 us
  Pallas kernels  65 us (97%)
  local copies, waits for them, and re-layouts  1.57 us (2%)
    pallas_call x1, Pallas kernels, fused(): pl.pallas_call(functools.partial(layer_kernel, zs), out_shape=jax.ShapeDt...  65 us
    unnamed x1, local copies, waits for them, and re-layouts  1.57 us

profile of v2, /device:TPU:1, one launch (start us, length us, event | category | flops | bytes accessed | tf_op | source)
XLA Modules:
  0.0 66.6 jit_solution(13099466200651371438)
XLA Ops:
  0.0 65.0 %shard_map.109 = bf16[32,2048]{1,0:T(8,128)(2,1)} custom-call(bf16[32,2048]{1,0:T(8,128)(2,1)} %tokens_ref.1, f32[1,2048]{1,0:T(1,128)} %bitcast.4, s32[8,32]{1,0:T(8,128)} %bitcast.6, f32[8,32]{1,0:T(8,128)} %bitcast.7, f32[1,2048]{1,0:T(1,128)} %bitcast.5, bf16[1,2048,1024]{2,1,0:T(8,128)(2,1)} %gate_hbm.1, bf16[1,2048,1024]{2,1,0:T(8,128)(2,1)} %up_hbm.1, ...), custom_call_target="tpu_custom_call" | custom-call | tf_op jit(solution)/shard_map/pallas_call | solution.py:366
  65.0 1.6 %copy.13 = bf16[32,2048]{1,0:T(8,128)(2,1)} copy(bf16[32,2048]{1,0:T(8,128)(2,1)} %shard_map.109) | data formatting | bytes 262144
